TPU v7x, 32 devices: a whole 2x2x4 slice. The times are simulated.
32 devices in a mesh: sp: 16 (over z, y, x), tp: 2 (over core).
Axes of the slice: x: 2, y: 2, z: 4, core: 2. Of those that a mesh axis runs over, the one named last changes fastest.
Arguments:
- resid: bfloat16 [4096, 2048], P('sp', 'tp'), may hold values from -6 to 6
- queries: bfloat16 [4096, 1024], P('sp', 'tp'), may hold values from -6 to 6
- keys_values: bfloat16 [8, 4096, 128], P('tp', 'sp'), may hold values from -6 to 6
- cum_gate: float32 [16, 4096], P('tp', 'sp'), as said below
- out_weight: bfloat16 [1024, 2048], P(None, 'tp'), may hold values from -1.5 to 1.5
- norm_gain: float32 [2048], replicated, may hold values from 0.1 to 1.9
- gate_weight: bfloat16 [2048, 5632], P('sp', 'tp'), may hold values from -0.125 to 0.125
- up_weight: bfloat16 [2048, 5632], P('sp', 'tp'), may hold values from -0.125 to 0.125
- conv_kernel: float32 [3, 2, 5632], P(None, None, 'tp'), may hold values from -3.5 to 3.5
- down_weight: bfloat16 [5632, 2048], P('tp', 'sp'), may hold values from -0.078125 to 0.078125
Outputs:
- layer_out: bfloat16 [4096, 2048], P('sp', 'tp')
Inputs may be any that keep to these rules, and one draw needn't show every extreme that they name: `cum_gate`: along positions each head's entries never increase.
All inputs are finite; a program needn't handle non-finite values.
Results may differ from a plain program's by a relative error of at most 0.015.
Values may be sent and summed in bfloat16 or wider, within the bound.
A program may use at most 128 MiB of HBM per device.

v0:
```python
import jax
import jax.numpy as jnp
from jax import lax
from jax.sharding import PartitionSpec as P

norm_eps = 1e-06


def from_behind(value, axis, by):
    size = lax.axis_size(axis)
    pairs = [(i, i + by) for i in range(size) if 0 <= i + by < size]
    return lax.ppermute(value, axis, pairs)


def attend(queries, keys_values, cum_gate, row_start):
    tok_rows = queries.shape[0]
    local_pairs = keys_values.shape[0]
    head_dim = keys_values.shape[2] // 2
    local_heads = cum_gate.shape[0]
    group_size = local_heads // local_pairs
    score_scale = head_dim ** (-0.5)
    query_heads = queries.reshape(tok_rows, local_pairs, group_size, head_dim)
    all_gates = lax.all_gather(cum_gate, "sp", axis=1, tiled=True)
    own_gates = lax.dynamic_slice_in_dim(all_gates, row_start, tok_rows, 1).reshape(
        local_pairs, group_size, tok_rows
    )
    query_pos = row_start + jnp.arange(tok_rows, dtype=jnp.int32)
    last_row = row_start + tok_rows - 1

    def add_block(state_now, key_block, offset):
        block_width = key_block.shape[1]
        key_part = key_block[:, :, :head_dim]
        values = key_block[:, :, head_dim:]
        key_gates = lax.dynamic_slice_in_dim(all_gates, offset, block_width, 1).reshape(
            local_pairs, group_size, block_width
        )
        scores = (
            jnp.einsum("tkgd,krd->kgtr", query_heads, key_part, preferred_element_type=jnp.float32)
            * score_scale
        )
        scores = scores + own_gates[:, :, :, None] - key_gates[:, :, None, :]
        visible = query_pos[:, None] >= (offset + jnp.arange(block_width, dtype=jnp.int32))[None, :]
        scores = jnp.where(visible, scores, -1e30)
        running_max, running_sum, weighted = state_now
        next_max = jnp.maximum(running_max, jnp.max(scores, axis=3))
        weights = jnp.where(visible, jnp.exp(scores - next_max[:, :, :, None]), 0.0)
        shrink = jnp.exp(running_max - next_max)
        running_sum = running_sum * shrink + jnp.sum(weights, axis=3)
        weighted = weighted * shrink[:, :, :, None] + jnp.einsum(
            "kgtr,krd->kgtd",
            weights.astype(jnp.bfloat16),
            values,
            preferred_element_type=jnp.float32,
        )
        return (next_max, running_sum, weighted)

    start_state = (
        jnp.full((local_pairs, group_size, tok_rows), -1e30, jnp.float32),
        jnp.zeros((local_pairs, group_size, tok_rows), jnp.float32),
        jnp.zeros((local_pairs, group_size, tok_rows, head_dim), jnp.float32),
    )
    arrived = lax.all_gather(keys_values, "sp", axis=1, tiled=True)
    arrived_rows = arrived.shape[1]
    block_rows = 512

    def fold_block(block_index, inner):
        block_start = block_index * block_rows
        key_block = lax.dynamic_slice_in_dim(arrived, block_index * block_rows, block_rows, 1)
        return lax.cond(
            block_start <= last_row,
            lambda current: add_block(current, key_block, block_start),
            lambda current: current,
            inner,
        )

    running_max, running_sum, weighted = lax.fori_loop(
        0, arrived_rows // block_rows, fold_block, start_state
    )
    result = (weighted / running_sum[:, :, :, None]).transpose(2, 0, 1, 3)
    return result.reshape(tok_rows, local_heads * head_dim).astype(jnp.bfloat16)


def local(
    resid,
    queries,
    keys_values,
    cum_gate,
    out_weight,
    norm_gain,
    gate_weight,
    up_weight,
    conv_kernel,
    down_weight,
):
    tok_rows = resid.shape[0]
    hidden_cols = gate_weight.shape[1]
    row_start = lax.axis_index("sp") * tok_rows
    attn = attend(queries, keys_values, cum_gate, row_start)
    branch = jnp.dot(
        lax.all_gather(attn, "tp", axis=1, tiled=True),
        out_weight,
        preferred_element_type=jnp.float32,
    )
    middle = (resid.astype(jnp.float32) + branch).astype(jnp.bfloat16)
    middle_f32 = middle.astype(jnp.float32)
    middle_full = lax.all_gather(middle, "tp", axis=1, tiled=True).astype(jnp.float32)
    inverse = lax.rsqrt(jnp.mean(middle_full * middle_full, axis=1, keepdims=True) + norm_eps)
    normed = (middle_full * inverse * norm_gain).astype(jnp.bfloat16)
    gate_sum = jnp.dot(
        normed,
        lax.all_gather(gate_weight, "sp", axis=0, tiled=True),
        preferred_element_type=jnp.float32,
    )
    up_sum = jnp.dot(
        normed,
        lax.all_gather(up_weight, "sp", axis=0, tiled=True),
        preferred_element_type=jnp.float32,
    )
    pre_gate = gate_sum.astype(jnp.bfloat16)
    pre_up = up_sum.astype(jnp.bfloat16)
    reach_back = conv_kernel.shape[0] - 1
    joined = jnp.concatenate([pre_gate, pre_up], axis=1)
    before = from_behind(joined[tok_rows - reach_back :], "sp", 1)
    padded = jnp.concatenate([before, joined], axis=0).astype(jnp.float32)
    kernel = conv_kernel.reshape(reach_back + 1, 2 * hidden_cols)
    mixed = jnp.zeros((tok_rows, 2 * hidden_cols), jnp.float32)
    for offset in range(reach_back + 1):
        mixed = mixed + kernel[offset][None, :] * padded[offset : offset + tok_rows]
    hidden = (jax.nn.silu(mixed[:, :hidden_cols]) * mixed[:, hidden_cols:]).astype(jnp.bfloat16)
    partials = jnp.dot(
        hidden,
        lax.all_gather(down_weight, "sp", axis=1, tiled=True),
        preferred_element_type=jnp.float32,
    )
    channel_out = lax.psum_scatter(
        partials.astype(jnp.bfloat16), "tp", scatter_dimension=1, tiled=True
    ).astype(jnp.float32)
    return (middle_f32 + channel_out).astype(jnp.bfloat16)


def solution(mesh):
    return jax.shard_map(
        local,
        mesh=mesh,
        in_specs=(
            P("sp", "tp"),
            P("sp", "tp"),
            P("tp", "sp", None),
            P("tp", "sp"),
            P(None, "tp"),
            P(),
            P("sp", "tp"),
            P("sp", "tp"),
            P(None, None, "tp"),
            P("tp", "sp"),
        ),
        out_specs=P("sp", "tp"),
        check_vma=False,
    )
```

profile of v0, /device:TPU:0, one launch (start us, length us, event | category | flops | bytes accessed | tf_op | source)
XLA Modules:
  0.0 685.5 jit_solution(4768735813569886703)
XLA Ops:
  6.5 1.9 copy.12
  8.5 0.0 all-gather.8.cloned.1.call-start
  8.6 1.8 copy.13
  10.4 43.6 %all_gather.22 = f32[8,4096]{1,0:T(8,128)S(1)} all-gather(f32[8,256]{1,0:T(8,128)} %param.17), channel_id=1, replica_groups=mesh['sp'=16,'tp'=2] {'sp'}, dimensions={1}, use_global_device_ids=true | all-gather | bytes 139264 | tf_op jit(solution)/shard_map/all_gather | solution.py:23
  54.0 46.1 %all-gather.6.cloned.1.call-done = bf16[4,4096,128]{1,2,0:T(8,128)(2,1)} async-done(((bf16[4,256,128]{1,2,0:T(8,128)(2,1)}), bf16[4,4096,128]{1,2,0:T(8,128)(2,1)}) %all-gather.6.cloned.1.call-update) | async-done | bytes 4194320 | tf_op jit(solution)/shard_map/all_gather | solution.py:62
  100.2 10.1 %while.18 = (s32[]{:T(128)}, f32[4,2,256]{2,1,0:T(2,128)S(1)}, f32[4,2,256]{2,1,0:T(2,128)S(1)}, f32[4,2,256,64]{2,3,1,0:T(8,128)S(1)}, s32[]{:T(128)}, /*index=...) while((s32[]{:T(128)}, f32[4,2,256]{2,1,0:T(2,128)S(1)}, ...), condition=%wide.region_5.6_spmd.clone, body=%wide.region_0.5_spmd.clone.sunk | while | flops 288756480 | bytes 32014712 | solution.py:76
  100.3 9.7 %conditional.3 = ((f32[4,2,256]{2,1,0:T(2,128)S(1)}, f32[4,2,256]{2,1,0:T(2,128)S(1)}, f32[4,2,256,64]{2,3,1,0:T(8,128)S(1)})) conditional(s32[]{:T(128)} %convert_element_type.103, (f32[4,2,256]{2,1,0:T(2,128)S(1)}, f32[4,2,256]{2,1,0:T(2,128)S(1)}, f32[4,2,256,64]{2,3,1,0:T(8,128)S(1)}) %tuple.53, (s32[]{:T(128)}, s32[]{:T(128)}, ...), branch_computations={%region_1.0_spmd, %region_2.4_spmd} | conditional | flops 288756480 | bytes 32013442 | solution.py:69
  100.3 0.1 broadcast_compare_fusion
  100.5 2.5 fusion.6
  103.0 2.0 copy-done.2
  105.0 1.5 fusion.5
  106.5 3.4 fusion.10
  110.4 2.2 all_gather.23
  112.6 1.5 fusion.27
  114.1 0.0 all-gather.10.cloned.1.call-start
  114.2 0.7 all-gather.10.cloned.1.call-update
  114.9 0.5 all-gather.12.cloned.1.call-update
  115.5 0.5 all-gather.14.cloned.1.call-update
  116.1 73.0 %all-gather.8.cloned.1.call-done = bf16[256,2048]{1,0:T(8,128)(2,1)} async-done(((bf16[256,1024]{1,0:T(8,128)(2,1)}), bf16[256,2048]{1,0:T(8,128)(2,1)}) %all-gather.8.cloned.1.call-update) | async-done | bytes 1048592 | tf_op jit(solution)/shard_map/all_gather | solution.py:106
  189.1 1.5 fusion.22
  190.6 143.9 %all-gather.10.cloned.1.call-done = bf16[2048,2816]{1,0:T(8,128)(2,1)} async-done(((bf16[128,2816]{1,0:T(8,128)(2,1)}), bf16[2048,2816]{1,0:T(8,128)(2,1)}) %all-gather.10.cloned.1.call-update) | async-done | bytes 11534352 | tf_op jit(solution)/shard_map/all_gather | solution.py:111
  334.5 7.8 %convolution_convert_fusion.1 = bf16[256,2816]{1,0:T(8,128)(2,1)S(1)} fusion(bf16[2048,2816]{1,0:T(8,128)(2,1)} %all-gather.10.cloned.1.call-done, bf16[256,2048]{1,0:T(8,128)(2,1)} %all-gather.8.cloned.1.call-done, f32[2048]{0:T(1024)S(1)} %copy-done.6, f32[256]{0:T(256)S(1)} %add_rsqrt_fusion), kind=kOutput, calls=%fused_computation.31 | convolution fusion | flops 2955608064 | bytes 14033920 | tf_op jit(solution)/shard_map/dot_general | solution.py:109
  342.3 134.4 %all-gather.12.cloned.1.call-done = bf16[2048,2816]{1,0:T(8,128)(2,1)} async-done(((bf16[128,2816]{1,0:T(8,128)(2,1)}), bf16[2048,2816]{1,0:T(8,128)(2,1)}) %all-gather.12.cloned.1.call-update) | async-done | bytes 11534352 | tf_op jit(solution)/shard_map/all_gather | solution.py:116
  476.7 7.8 %convolution_convert_fusion = bf16[256,2816]{1,0:T(8,128)(2,1)S(1)} fusion(bf16[2048,2816]{1,0:T(8,128)(2,1)} %all-gather.12.cloned.1.call-done, bf16[256,2048]{1,0:T(8,128)(2,1)} %all-gather.8.cloned.1.call-done, f32[2048]{0:T(1024)S(1)} %copy-done.6, f32[256]{0:T(256)S(1)} %add_rsqrt_fusion), kind=kOutput, calls=%fused_computation.30 | convolution fusion | flops 2955608064 | bytes 14033920 | tf_op jit(solution)/shard_map/dot_general | solution.py:114
  484.6 3.4 collective-permute-start
  488.0 1.6 collective-permute-done
  489.7 0.8 maximum_convert_fusion
  490.5 3.5 fusion.19
  493.9 165.6 %all-gather.14.cloned.1.call-done = bf16[2816,2048]{1,0:T(8,128)(2,1)} async-done(((bf16[2816,128]{1,0:T(8,128)(2,1)}), bf16[2816,2048]{1,0:T(8,128)(2,1)}) %all-gather.14.cloned.1.call-update) | async-done | bytes 11534352 | tf_op jit(solution)/shard_map/all_gather | solution.py:132
  659.5 10.4 %convolution_convert_fusion.2 = bf16[256,2048]{1,0:T(8,128)(2,1)} fusion(bf16[2816,2048]{1,0:T(8,128)(2,1)} %all-gather.14.cloned.1.call-done, f32[256,5632]{1,0:T(8,128)} %fusion.19), kind=kOutput, calls=%fused_computation.37 | convolution fusion | flops 2957639680 | bytes 18350080 | tf_op jit(solution)/shard_map/dot_general | solution.py:130
  669.9 6.7 reduce-scatter.2.cloned.1.call-done
  676.6 2.0 add_convert_fusion
  (54 shorter events, 0.6 us)
Async XLA Ops:
  6.5 106.0 %copy-start = (bf16[1024,1024]{1,0:T(8,128)(2,1)S(1)}, bf16[1024,1024]{1,0:T(8,128)(2,1)}, u32[]{:S(2)}) copy-start(bf16[1024,1024]{1,0:T(8,128)(2,1)} %param.18) | copy-start | bytes 6291460
  6.5 93.6 %all-gather.6.cloned.1.call-start = ((), (), s32[]{:S(2)}) async-start(), calls=%async_computation.1 | async-start | bytes 4456448 | tf_op jit(solution)/shard_map/all_gather | solution.py:62
  8.5 180.6 %all-gather.8.cloned.1.call-start = ((), (), s32[]{:S(2)}) async-start(), calls=%async_computation.2 | async-start | bytes 1572864 | tf_op jit(solution)/shard_map/all_gather | solution.py:106
  100.2 12.4 %copy-start.4 = (bf16[256,1024]{1,0:T(8,128)(2,1)S(1)}, bf16[256,1024]{1,0:T(8,128)(2,1)}, u32[]{:S(2)}) copy-start(bf16[256,1024]{1,0:T(8,128)(2,1)} %param.14) | copy-start | bytes 1572868
  103.0 2.0 copy-start.2
  110.4 224.1 %copy-start.6 = (f32[2048]{0:T(1024)S(1)}, f32[2048]{0:T(1024)}, u32[]{:S(2)}) copy-start(f32[2048]{0:T(1024)} %param.19) | copy-start | bytes 24580
  114.1 220.3 %all-gather.10.cloned.1.call-start = ((), (), s32[]{:S(2)}) async-start(), calls=%async_computation.3 | async-start | bytes 12255232 | tf_op jit(solution)/shard_map/all_gather | solution.py:111
  114.9 361.8 %all-gather.12.cloned.1.call-start = ((), (), s32[]{:S(2)}) async-start(), calls=%async_computation.4 | async-start | bytes 12255232 | tf_op jit(solution)/shard_map/all_gather | solution.py:116
  115.4 544.1 %all-gather.14.cloned.1.call-start = ((), (), s32[]{:S(2)}) async-start(), calls=%async_computation.5 | async-start | bytes 12255232 | tf_op jit(solution)/shard_map/all_gather | solution.py:132
  116.0 560.6 %reduce-scatter.2.cloned.1.call-start = ((), (), s32[]{:S(2)}) async-start(), calls=%async_computation.6 | async-start | bytes 1572864 | tf_op jit(solution)/shard_map/reduce_scatter | solution.py:135
  342.3 145.6 %copy-start.5 = (f32[3,2,2816]{2,1,0:T(2,128)S(1)}, f32[3,2,2816]{2,1,0:T(2,128)}, u32[]{:S(2)}) copy-start(f32[3,2,2816]{2,1,0:T(2,128)} %param.22) | copy-start | bytes 202756
  484.6 5.1 collective-permute-start
  493.9 182.7 %copy-start.3 = (bf16[256,1024]{1,0:T(8,128)(2,1)S(1)}, bf16[256,1024]{1,0:T(8,128)(2,1)}, u32[]{:S(2)}) copy-start(bf16[256,1024]{1,0:T(8,128)(2,1)} %fusion.27) | copy-start | bytes 1572868
  659.5 19.2 %copy-start.1 = (bf16[1024,1024]{1,0:T(8,128)(2,1)S(1)}, bf16[1024,1024]{1,0:T(8,128)(2,1)}, u32[]{:S(2)}) copy-start(bf16[1024,1024]{1,0:T(8,128)(2,1)} %param.18) | copy-start | bytes 6291460
Sparse Core Ops, SparseCore 0:
  10.1 90.0 all-gather.5
  114.2 74.7 all-gather.7
  191.8 142.5 all-gather.9
  337.1 139.5 all-gather.11
  479.3 180.2 all-gather.13
  670.0 6.5 reduce-scatter.1
where the time goes:
time: 686 us
  waiting for transfers between devices  573 us (84%)
  blocking collectives  45.8 us (7%)
  matrix products  33.4 us (5%)
  between operations  13.6 us (2%)
  other arithmetic  9.58 us (1%)
    all_gather x1, waiting for transfers between devices, local(): lax.all_gather(down_weight, 'sp', axis=1, tiled=True)  166 us
    all_gather x1, waiting for transfers between devices, local(): lax.all_gather(gate_weight, 'sp', axis=0, tiled=True)  144 us
    all_gather x1, waiting for transfers between devices, local(): lax.all_gather(up_weight, 'sp', axis=0, tiled=True)  134 us
    all_gather x1, waiting for transfers between devices, local(): lax.all_gather(middle, 'tp', axis=1, tiled=True).astype(jnp.float32)  73 us
    all_gather x1, waiting for transfers between devices, attend(): arrived = lax.all_gather(keys_values, 'sp', axis=1, tiled=True)  46.1 us
    all_gather x1, blocking collectives, attend(): all_gates = lax.all_gather(cum_gate, 'sp', axis=1, tiled=True)  43.6 us
  transfers between devices with their start and end apart: 7, of which 7 were waited for; matrix products, arithmetic and copies ran while one was open for 3% of the time, Pallas kernels for 0%

commit v1 on v0

--- a/solution.py
+++ b/solution.py
@@ -4,6 +4,10 @@
 from jax.sharding import PartitionSpec as P
 
 norm_eps = 1e-06
+
+
+def seats_all_review(frame, mesh_ax):
+    return jnp.concatenate(lax.all_gather(frame, axis_name=mesh_ax), axis=1)
 
 
 def from_behind(value, axis, by):
@@ -128,9 +132,7 @@
         mixed = mixed + kernel[offset][None, :] * padded[offset : offset + tok_rows]
     hidden = (jax.nn.silu(mixed[:, :hidden_cols]) * mixed[:, hidden_cols:]).astype(jnp.bfloat16)
     partials = jnp.dot(
-        hidden,
-        lax.all_gather(down_weight, "sp", axis=1, tiled=True),
-        preferred_element_type=jnp.float32,
+        hidden, seats_all_review(down_weight, "sp"), preferred_element_type=jnp.float32
     )
     channel_out = lax.psum_scatter(
         partials.astype(jnp.bfloat16), "tp", scatter_dimension=1, tiled=True

time: 686 us -> 662 us (0.965)
  waiting for transfers between devices: 573 us -> 537 us
  local copies, waits for them, and re-layouts: 5.91 us -> 20.9 us
    all_gather x1, waiting for transfers between devices: 166 us -> 131 us  [seats_all_review(): return jnp.concatenate(lax.all_gather(frame, axis_name=mesh_ax), axis=1)]
    reshape x0 -> x1, local copies, waits for them, and re-layouts: none -> 15 us  [seats_all_review(): return jnp.concatenate(lax.all_gather(frame, axis_name=mesh_ax), axis=1)]
    all_gather x1, waiting for transfers between devices: 144 us -> 134 us  [local(): lax.all_gather(gate_weight, 'sp', axis=0, tiled=True)]
    all_gather x1, waiting for transfers between devices: 134 us -> 144 us  [local(): lax.all_gather(up_weight, 'sp', axis=0, tiled=True)]
  transfers between devices with their start and end apart: 7 -> 7, of which waited for: 7 -> 6; matrix products, arithmetic and copies ran while one was open for 3% -> 5% of each run, Pallas kernels for 0% -> 0%
where the time goes in v1:
time: 662 us; the launch traced here: 661 us
  waiting for transfers between devices  537 us (81%)
  blocking collectives  45.8 us (7%)
  matrix products  31.7 us (5%)
  local copies, waits for them, and re-layouts  20.9 us (3%)
  between operations  13.7 us (2%)
  other arithmetic  7.84 us (1%)
    all_gather x1, waiting for transfers between devices, local(): lax.all_gather(up_weight, 'sp', axis=0, tiled=True)  144 us
    all_gather x1, waiting for transfers between devices, local(): lax.all_gather(gate_weight, 'sp', axis=0, tiled=True)  134 us
    all_gather x1, waiting for transfers between devices, seats_all_review(): return jnp.concatenate(lax.all_gather(frame, axis_name=mesh_ax), axis=1)  131 us
    all_gather x1, waiting for transfers between devices, local(): lax.all_gather(middle, 'tp', axis=1, tiled=True).astype(jnp.float32)  72.7 us
    all_gather x1, waiting for transfers between devices, attend(): arrived = lax.all_gather(keys_values, 'sp', axis=1, tiled=True)  46.1 us
    all_gather x1, blocking collectives, attend(): all_gates = lax.all_gather(cum_gate, 'sp', axis=1, tiled=True)  43.6 us
    reshape x1, local copies, waits for them, and re-layouts, seats_all_review(): return jnp.concatenate(lax.all_gather(frame, axis_name=mesh_ax), axis=1)  15 us
  transfers between devices with their start and end apart: 7, of which 6 were waited for; matrix products, arithmetic and copies ran while one was open for 5% of the time, Pallas kernels for 0%

profile of v1, /device:TPU:0, one launch (start us, length us, event | category | flops | bytes accessed | tf_op | source)
XLA Modules:
  0.0 660.8 jit_solution(4545531902259402513)
XLA Ops:
  6.5 1.9 copy.18
  8.5 0.0 all-gather.9.cloned.1.call-start
  8.6 1.8 copy.19
  10.4 43.6 %all_gather.25 = f32[8,4096]{1,0:T(8,128)S(1)} all-gather(f32[8,256]{1,0:T(8,128)} %param.17), channel_id=1, replica_groups=mesh['sp'=16,'tp'=2] {'sp'}, dimensions={1}, use_global_device_ids=true | all-gather | bytes 139264 | tf_op jit(solution)/shard_map/all_gather | solution.py:27
  54.0 46.1 %all-gather.7.cloned.1.call-done = bf16[4,4096,128]{1,2,0:T(8,128)(2,1)} async-done(((bf16[4,256,128]{1,2,0:T(8,128)(2,1)}), bf16[4,4096,128]{1,2,0:T(8,128)(2,1)}) %all-gather.7.cloned.1.call-update) | async-done | bytes 4194320 | tf_op jit(solution)/shard_map/all_gather | solution.py:66
  100.2 10.1 %while.18 = (s32[]{:T(128)}, f32[4,2,256]{2,1,0:T(2,128)S(1)}, f32[4,2,256]{2,1,0:T(2,128)S(1)}, f32[4,2,256,64]{2,3,1,0:T(8,128)S(1)}, s32[]{:T(128)}, /*index=...) while((s32[]{:T(128)}, f32[4,2,256]{2,1,0:T(2,128)S(1)}, ...), condition=%wide.region_5.6_spmd.clone, body=%wide.region_0.5_spmd.clone.sunk | while | flops 288756480 | bytes 32014712 | solution.py:80
  100.3 9.6 %conditional.3 = ((f32[4,2,256]{2,1,0:T(2,128)S(1)}, f32[4,2,256]{2,1,0:T(2,128)S(1)}, f32[4,2,256,64]{2,3,1,0:T(8,128)S(1)})) conditional(s32[]{:T(128)} %convert_element_type.103, (f32[4,2,256]{2,1,0:T(2,128)S(1)}, f32[4,2,256]{2,1,0:T(2,128)S(1)}, f32[4,2,256,64]{2,3,1,0:T(8,128)S(1)}) %tuple.53, (s32[]{:T(128)}, s32[]{:T(128)}, ...), branch_computations={%region_1.0_spmd, %region_2.4_spmd} | conditional | flops 288756480 | bytes 32013442 | solution.py:73
  100.3 0.1 broadcast_compare_fusion
  100.5 2.4 fusion.6
  103.0 2.0 copy-done.2
  105.0 1.5 fusion.5
  106.5 3.4 fusion.10
  110.3 0.1 divide_convert_fusion
  110.4 2.2 all_gather.26
  112.5 1.5 fusion.27
  114.1 0.7 all-gather.13.cloned.1.call-update
  114.9 0.5 all-gather.11.cloned.1.call-update
  115.4 0.5 all-gather.15.cloned.1.call-update
  116.0 72.7 %all-gather.9.cloned.1.call-done = bf16[256,2048]{1,0:T(8,128)(2,1)} async-done(((bf16[256,1024]{1,0:T(8,128)(2,1)}), bf16[256,2048]{1,0:T(8,128)(2,1)}) %all-gather.9.cloned.1.call-update) | async-done | bytes 1048592 | tf_op jit(solution)/shard_map/all_gather | solution.py:110
  188.8 1.5 fusion.22
  190.3 143.9 %all-gather.13.cloned.1.call-done = bf16[2048,2816]{1,0:T(8,128)(2,1)} async-done(((bf16[128,2816]{1,0:T(8,128)(2,1)}), bf16[2048,2816]{1,0:T(8,128)(2,1)}) %all-gather.13.cloned.1.call-update) | async-done | bytes 11534352 | tf_op jit(solution)/shard_map/all_gather | solution.py:120
  334.2 7.8 %convolution_convert_fusion = bf16[256,2816]{1,0:T(8,128)(2,1)S(1)} fusion(bf16[2048,2816]{1,0:T(8,128)(2,1)} %all-gather.13.cloned.1.call-done, bf16[256,2048]{1,0:T(8,128)(2,1)} %all-gather.9.cloned.1.call-done, f32[2048]{0:T(1024)S(1)} %copy-done.6, f32[256]{0:T(256)S(1)} %add_rsqrt_fusion), kind=kOutput, calls=%fused_computation.30 | convolution fusion | flops 2955608064 | bytes 14033920 | tf_op jit(solution)/shard_map/dot_general | solution.py:118
  342.0 134.4 %all-gather.11.cloned.1.call-done = bf16[2048,2816]{1,0:T(8,128)(2,1)} async-done(((bf16[128,2816]{1,0:T(8,128)(2,1)}), bf16[2048,2816]{1,0:T(8,128)(2,1)}) %all-gather.11.cloned.1.call-update) | async-done | bytes 11534352 | tf_op jit(solution)/shard_map/all_gather | solution.py:115
  476.4 7.8 %convolution_convert_fusion.1 = bf16[256,2816]{1,0:T(8,128)(2,1)S(1)} fusion(bf16[2048,2816]{1,0:T(8,128)(2,1)} %all-gather.11.cloned.1.call-done, bf16[256,2048]{1,0:T(8,128)(2,1)} %all-gather.9.cloned.1.call-done, f32[2048]{0:T(1024)S(1)} %copy-done.6, f32[256]{0:T(256)S(1)} %add_rsqrt_fusion), kind=kOutput, calls=%fused_computation.31 | convolution fusion | flops 2955608064 | bytes 14033920 | tf_op jit(solution)/shard_map/dot_general | solution.py:113
  484.3 3.4 collective-permute-start
  487.7 131.2 %all-gather.15.cloned.1.call-done = bf16[45056,128]{1,0:T(8,128)(2,1)} async-done(((bf16[2816,128]{1,0:T(8,128)(2,1)}), bf16[45056,128]{1,0:T(8,128)(2,1)}) %all-gather.15.cloned.1.call-update) | async-done | bytes 11534352 | tf_op jit(solution)/shard_map/all_gather | solution.py:10
  618.9 15.0 %copy.20 = bf16[2816,16,128]{0,2,1:T(8,128)(2,1)} copy(bf16[2816,16,128]{2,0,1:T(8,128)(2,1)} %bitcast.47) | data formatting | bytes 23068672 | tf_op jit(solution)/shard_map/reshape | solution.py:10
  633.9 0.8 maximum_convert_fusion
  634.8 1.7 fusion.19
  636.5 8.7 %convolution_convert_fusion.2 = bf16[256,2048]{1,0:T(8,128)(2,1)} fusion(bf16[2816,2048]{0,1:T(8,128)(2,1)} %bitcast.48, f32[256,5632]{1,0:T(8,128)S(1)} %fusion.19), kind=kOutput, calls=%fused_computation.37 | convolution fusion | flops 2957639680 | bytes 18350080 | tf_op jit(solution)/shard_map/dot_general | solution.py:134
  645.2 6.7 %reduce-scatter.2.cloned.1.call-done = bf16[256,1024]{1,0:T(8,128)(2,1)} async-done(((bf16[256,2048]{1,0:T(8,128)(2,1)}), bf16[256,1024]{1,0:T(8,128)(2,1)}) %reduce-scatter.2.cloned.1.call-update) | async-done | bytes 524304 | tf_op jit(solution)/shard_map/reduce_scatter | solution.py:137
  652.0 2.0 add_convert_fusion
  (55 shorter events, 0.6 us)
Async XLA Ops:
  6.5 106.0 %copy-start = (bf16[1024,1024]{1,0:T(8,128)(2,1)S(1)}, bf16[1024,1024]{1,0:T(8,128)(2,1)}, u32[]{:S(2)}) copy-start(bf16[1024,1024]{1,0:T(8,128)(2,1)} %param.18) | copy-start | bytes 6291460
  6.5 93.6 %all-gather.7.cloned.1.call-start = ((), (), s32[]{:S(2)}) async-start(), calls=%async_computation.1 | async-start | bytes 4456448 | tf_op jit(solution)/shard_map/all_gather | solution.py:66
  8.5 180.3 %all-gather.9.cloned.1.call-start = ((), (), s32[]{:S(2)}) async-start(), calls=%async_computation.2 | async-start | bytes 1572864 | tf_op jit(solution)/shard_map/all_gather | solution.py:110
  100.2 12.3 %copy-start.4 = (bf16[256,1024]{1,0:T(8,128)(2,1)S(1)}, bf16[256,1024]{1,0:T(8,128)(2,1)}, u32[]{:S(2)}) copy-start(bf16[256,1024]{1,0:T(8,128)(2,1)} %param.14) | copy-start | bytes 1572868
  103.0 2.0 copy-start.2
  110.3 223.8 %copy-start.6 = (f32[2048]{0:T(1024)S(1)}, f32[2048]{0:T(1024)}, u32[]{:S(2)}) copy-start(f32[2048]{0:T(1024)} %param.19) | copy-start | bytes 24580
  114.1 220.1 %all-gather.13.cloned.1.call-start = ((), (), s32[]{:S(2)}) async-start(), calls=%async_computation.4 | async-start | bytes 12255232 | tf_op jit(solution)/shard_map/all_gather | solution.py:120
  114.8 361.6 %all-gather.11.cloned.1.call-start = ((), (), s32[]{:S(2)}) async-start(), calls=%async_computation.3 | async-start | bytes 12255232 | tf_op jit(solution)/shard_map/all_gather | solution.py:115
  115.4 503.5 %all-gather.15.cloned.1.call-start = ((), (), s32[]{:S(2)}) async-start(), calls=%async_computation.6 | async-start | bytes 12255232 | tf_op jit(solution)/shard_map/all_gather | solution.py:10
  116.0 536.0 %reduce-scatter.2.cloned.1.call-start = ((), (), s32[]{:S(2)}) async-start(), calls=%async_computation.5 | async-start | bytes 1572864 | tf_op jit(solution)/shard_map/reduce_scatter | solution.py:137
  342.0 145.6 %copy-start.5 = (f32[3,2,2816]{2,1,0:T(2,128)S(1)}, f32[3,2,2816]{2,1,0:T(2,128)}, u32[]{:S(2)}) copy-start(f32[3,2,2816]{2,1,0:T(2,128)} %param.22) | copy-start | bytes 202756
  484.3 149.7 %collective-permute-start = (bf16[2,5632]{1,0:T(2,128)(2,1)S(1)}, bf16[2,5632]{1,0:T(2,128)(2,1)S(1)}, u32[]{:S(2)}, u32[]{:S(2)}) collective-permute-start(bf16[2,5632]{1,0:T(2,128)(2,1)S(1)} %pad_maximum_fusion), channel_id=1, source_target_pairs={{0,2},{2,4},{4,6},{6,8},{8,10},{10,12},{12,14},{14,16},{16,18},{18... | collective-permute-start | bytes 67592 | tf_op jit(solution)/shard_map/ppermute | solution.py:16
  636.5 15.5 %copy-start.3 = (bf16[256,1024]{1,0:T(8,128)(2,1)S(1)}, bf16[256,1024]{1,0:T(8,128)(2,1)}, u32[]{:S(2)}) copy-start(bf16[256,1024]{1,0:T(8,128)(2,1)} %fusion.27) | copy-start | bytes 1572868
  636.5 17.5 %copy-start.1 = (bf16[1024,1024]{1,0:T(8,128)(2,1)S(1)}, bf16[1024,1024]{1,0:T(8,128)(2,1)}, u32[]{:S(2)}) copy-start(bf16[1024,1024]{1,0:T(8,128)(2,1)} %param.18) | copy-start | bytes 6291460
Sparse Core Ops, SparseCore 0:
  10.1 90.0 all-gather.6
  114.2 74.5 all-gather.8
  191.5 142.5 all-gather.12
  336.8 139.5 all-gather.10
  479.0 139.8 all-gather.14
  645.4 6.5 reduce-scatter.1
